TPU v7x, 256 devices: a whole 4x4x8 slice. The times are simulated.
256 devices in a mesh: ep: 32 (over z, x), tp: 8 (over y, core).
Axes of the slice: x: 4, y: 4, z: 8, core: 2. Of those that a mesh axis runs over, the one named last changes fastest.
Arguments:
- stream: bfloat16 [512, 4096], P(None, 'ep'), may hold values from -6.5 to 6.5
- norm_gain: float32 [4096], P('ep'), may hold values from 0.1 to 1.9
- w_query: bfloat16 [4096, 2048], P('ep', 'tp'), may hold values from -0.09375 to 0.09375
- w_key: bfloat16 [4096, 1024], P('ep', 'tp'), may hold values from -0.09375 to 0.09375
- w_value: bfloat16 [4096, 1024], P('ep', 'tp'), may hold values from -0.09375 to 0.09375
- break_offset: float32 [16], P('tp'), may hold values from -10 to -2
- cache_keys: bfloat16 [512, 1024, 8, 128], P('ep', None, 'tp'), may hold values from -6 to 6
- cache_values: bfloat16 [512, 1024, 8, 128], P('ep', None, 'tp'), may hold values from -6 to 6
- lengths: int32 [512], P('ep'), may hold values from 128 to 1024
- w_output: bfloat16 [2048, 4096], P('tp', 'ep'), may hold values from -0.125 to 0.125
- head_gain: float32 [2048], P('tp'), may hold values from 0.1 to 1.9
- ffn_gain: float32 [4096], P('ep'), may hold values from 0.1 to 1.9
- route_experts: int32 [512, 2], replicated, may hold values from 0 to 31, all different within a row; in each aligned block of 512 rows (0 to 511, 512 to 1023, ...) at most 64 rows name the same one
- route_weights: float32 [512, 2], replicated, may hold values from 0.1 to 1
- expert_gate: bfloat16 [32, 4096, 1024], P('ep', None, 'tp'), may hold values from -0.09375 to 0.09375
- expert_up: bfloat16 [32, 4096, 1024], P('ep', None, 'tp'), may hold values from -0.09375 to 0.09375
- expert_down: bfloat16 [32, 1024, 4096], P('ep', 'tp'), may hold values from -0.1875 to 0.1875
- dense_gate: bfloat16 [4096, 4096], P('ep', 'tp'), may hold values from -0.09375 to 0.09375
- dense_up: bfloat16 [4096, 4096], P('ep', 'tp'), may hold values from -0.09375 to 0.09375
- dense_down: bfloat16 [4096, 4096], P('tp', 'ep'), may hold values from -0.09375 to 0.09375
- mix_gain: float32 [4096], P('ep'), may hold values from 0.1 to 1.9
Outputs:
- mixed_out: bfloat16 [512, 4096], P(None, 'ep')
- key_rows: bfloat16 [512, 1024], P('ep', 'tp')
- value_rows: bfloat16 [512, 1024], P('ep', 'tp')
Inputs may be any that keep to these rules, and one draw needn't show every extreme that they name: `route_experts`: in the whole batch no expert is named by more than 64 pairs, a bound that some block reaches; the 2 experts of a token differ.
All inputs are finite; a program needn't handle non-finite values.
Results may differ from a plain program's by a relative error of at most 0.025.
Values may be sent and summed in bfloat16 or wider, within the bound.
A program may use at most 64 MiB of HBM per device.

v0:
```python
import jax
import jax.numpy as jnp
from jax import lax
from jax.sharding import PartitionSpec as P

EPSILON = 1e-06


def sent_to_all(x, axis):
    size = lax.axis_size(axis)
    return lax.all_to_all(jnp.broadcast_to(x[None], (size, *x.shape)), axis, 0, 0, tiled=True)


def taken_together(x, axis):
    return sent_to_all(x, axis).sum(axis=0)


def split_up(x, dim, size):
    lengths = x.shape
    blocks = x.reshape(*lengths[:dim], size, lengths[dim] // size, *lengths[dim + 1 :])
    return jnp.moveaxis(blocks, dim, 0)


def sent_and_summed(x, axis, dim):
    blocks = split_up(x, dim, lax.axis_size(axis))
    arrived = lax.all_to_all(blocks, axis, split_axis=0, concat_axis=0, tiled=True)
    return arrived.astype(jnp.float32).sum(axis=0)


def joined_along(blocks, dim):
    blocks = jnp.moveaxis(blocks, 0, dim)
    lengths = blocks.shape
    return blocks.reshape(*lengths[:dim], lengths[dim] * lengths[dim + 1], *lengths[dim + 2 :])


def gather_directly(x, axis, dim):
    return joined_along(sent_to_all(x, axis), dim)


def of_everyone(x, axis):
    return sent_to_all(x, axis).astype(jnp.float32).sum(axis=0)


def rms_scale(values, gain_vec, model_width):
    squares = taken_together(jnp.sum(values * values, axis=1), "ep")
    return values * lax.rsqrt(squares / model_width + EPSILON)[:, None] * gain_vec[None, :]


def to_heads(normed, weights):
    return sent_and_summed(
        jnp.dot(normed, weights, preferred_element_type=jnp.float32).astype(jnp.bfloat16), "ep", 0
    )


def from_heads(values, weights):
    partial_value = jnp.dot(
        gather_directly(values, "ep", 0), weights, preferred_element_type=jnp.float32
    )
    return (
        of_everyone(partial_value.astype(jnp.bfloat16), "tp")
        .astype(jnp.float32)
        .astype(jnp.bfloat16)
    )


def expert_terms(inputs, gate_w, up_w, down_w):
    gate_val = jnp.einsum("ecd,edf->ecf", inputs, gate_w, preferred_element_type=jnp.float32)
    up_val = jnp.einsum("ecd,edf->ecf", inputs, up_w, preferred_element_type=jnp.float32)
    hidden = (jax.nn.silu(gate_val) * up_val).astype(jnp.bfloat16)
    return jnp.einsum("ecf,efd->ecd", hidden, down_w, preferred_element_type=jnp.float32)


def slot_table(route_experts, experts, capacity):
    chosen = route_experts.reshape(-1)
    onehot = (chosen[:, None] == jnp.arange(experts, dtype=jnp.int32)[None, :]).astype(jnp.int32)
    earlier = jnp.cumsum(onehot, axis=0) - onehot
    rank_in = jnp.sum(earlier * onehot, axis=1)
    slot_ids = chosen * capacity + rank_in
    owners = jnp.arange(chosen.shape[0], dtype=jnp.int32) // route_experts.shape[1]
    filled = (
        jnp.full((experts * capacity,), route_experts.shape[0], jnp.int32).at[slot_ids].set(owners)
    )
    return (slot_ids, filled)


def per_device(
    stream,
    norm_gain,
    w_query,
    w_key,
    w_value,
    break_offset,
    cache_keys,
    cache_values,
    lengths,
    w_output,
    head_gain,
    ffn_gain,
    route_experts,
    route_weights,
    expert_gate,
    expert_up,
    expert_down,
    dense_gate,
    dense_up,
    dense_down,
    mix_gain,
):
    model_width = stream.shape[1] * lax.axis_size("ep")
    block_width = stream.shape[1]
    seq_count = lengths.shape[0]
    kv_local = cache_keys.shape[2]
    head_dim = cache_keys.shape[3]
    heads_local = break_offset.shape[0]
    group_size = heads_local // kv_local
    cache_len = cache_keys.shape[1]
    streamf = stream.astype(jnp.float32)
    normed = rms_scale(streamf, norm_gain, model_width).astype(jnp.bfloat16)
    projected = to_heads(normed, jnp.concatenate([w_query, w_key, w_value], axis=1))
    q_width = w_query.shape[1]
    k_width = w_key.shape[1]
    queries = (
        projected[:, :q_width]
        .astype(jnp.bfloat16)
        .reshape(seq_count, kv_local, group_size, head_dim)
    )
    key_rows = projected[:, q_width : q_width + k_width].astype(jnp.bfloat16)
    value_rows = projected[:, q_width + k_width :].astype(jnp.bfloat16)
    scores = jnp.einsum("skgd,slkd->skgl", queries, cache_keys, preferred_element_type=jnp.float32)
    scores = (
        scores * head_dim ** (-0.5) + break_offset.reshape(kv_local, group_size)[None, :, :, None]
    )
    in_cache = (jnp.arange(cache_len, dtype=jnp.int32)[None, :] < lengths[:, None])[
        :, None, None, :
    ]
    failed = jnp.where(in_cache, jax.nn.log_sigmoid(-scores), 0.0)
    later_sum = lax.cumsum(failed, axis=3, reverse=True) - failed
    weights = jnp.where(in_cache, jnp.exp(jax.nn.log_sigmoid(scores) + later_sum), 0.0).astype(
        jnp.bfloat16
    )
    attended = jnp.einsum(
        "skgl,slkd->skgd", weights, cache_values, preferred_element_type=jnp.float32
    )
    gains = head_gain.reshape(kv_local, group_size, head_dim)[None]
    normalized = (
        attended * lax.rsqrt(jnp.mean(attended * attended, axis=3, keepdims=True) + EPSILON) * gains
    )
    head_out = normalized.astype(jnp.bfloat16).reshape(seq_count, heads_local * head_dim)
    attn_out = from_heads(head_out, w_output)
    residual = streamf + attn_out.astype(jnp.float32)
    normed_ffn = rms_scale(residual, ffn_gain, model_width).astype(jnp.bfloat16)
    dense_width = dense_gate.shape[1]
    gate_up = to_heads(normed_ffn, jnp.concatenate([dense_gate, dense_up], axis=1))
    dense_hidden = (jax.nn.silu(gate_up[:, :dense_width]) * gate_up[:, dense_width:]).astype(
        jnp.bfloat16
    )
    dense_out = from_heads(dense_hidden, dense_down)
    experts = expert_gate.shape[0] * lax.axis_size("ep")
    capacity = 2 * seq_count * route_experts.shape[1] // expert_gate.shape[0]
    slot_ids, filled = slot_table(route_experts, experts, capacity)
    padded = jnp.concatenate([normed_ffn, jnp.zeros((1, block_width), jnp.bfloat16)], axis=0)
    outgoing = padded[filled].reshape(experts, capacity, block_width)
    slot_share = capacity // lax.axis_size("tp")
    own_slots = lax.dynamic_slice_in_dim(outgoing, lax.axis_index("tp") * slot_share, slot_share, 1)
    arrived = lax.all_to_all(own_slots, "ep", split_axis=0, concat_axis=2, tiled=True)
    gathered = lax.all_gather(arrived, "tp", axis=1, tiled=True)
    partial_value = expert_terms(gathered, expert_gate, expert_up, expert_down)
    summed = sent_and_summed(partial_value.astype(jnp.bfloat16), "tp", 1).astype(jnp.bfloat16)
    came_back = lax.all_to_all(summed, "ep", split_axis=2, concat_axis=0, tiled=True)
    returned = gather_directly(came_back, "tp", 1)
    picked = returned.reshape(experts * capacity, block_width)[slot_ids]
    picked = picked.reshape(route_experts.shape[0], route_experts.shape[1], block_width).astype(
        jnp.float32
    )
    shares = route_weights / jnp.sum(route_weights, axis=1, keepdims=True)
    moe_out = jnp.sum(picked * shares[:, :, None], axis=1)
    mixed_out = (residual + moe_out + mix_gain[None, :] * dense_out.astype(jnp.float32)).astype(
        jnp.bfloat16
    )
    return (mixed_out, key_rows, value_rows)


def solution(mesh):
    in_specs = (
        P(None, "ep"),
        P("ep"),
        P("ep", "tp"),
        P("ep", "tp"),
        P("ep", "tp"),
        P("tp"),
        P("ep", None, "tp", None),
        P("ep", None, "tp", None),
        P("ep"),
        P("tp", "ep"),
        P("tp"),
        P("ep"),
        P(),
        P(),
        P("ep", None, "tp"),
        P("ep", None, "tp"),
        P("ep", "tp", None),
        P("ep", "tp"),
        P("ep", "tp"),
        P("tp", "ep"),
        P("ep"),
    )
    out_specs = (P(None, "ep"), P("ep", "tp"), P("ep", "tp"))
    return jax.shard_map(
        per_device, mesh=mesh, in_specs=in_specs, out_specs=out_specs, check_vma=False
    )
```

profile of v0, /device:TPU:1, one launch (start us, length us, event | category | flops | bytes accessed | tf_op | source)
XLA Modules:
  0.0 309.1 jit_solution(11907331791318313063)
XLA Ops:
  0.6 1.1 fusion.21
  1.8 20.5 %all_to_all.85 = f32[32,1,512]{2,1,0:T(1,128)S(1)} all-to-all(f32[32,1,512]{2,1,0:T(1,128)S(1)} %broadcast_in_dim.37), channel_id=1, replica_groups=mesh['ep'=32,'tp'=8] {'ep'}, dimensions={0} | all-to-all | bytes 131072 | tf_op jit(solution)/shard_map/all_to_all | solution.py:11
  22.4 2.1 convolution_convert_fusion.2
  24.5 3.9 %all-to-all-start.1 = ((bf16[32,16,512]{2,1,0:T(8,128)(2,1)}), bf16[32,16,512]{2,1,0:T(8,128)(2,1)S(1)}, u32[]{:S(2)}, u32[]{:S(2)}) async-start(bf16[32,16,512]{2,1,0:T(8,128)(2,1)} %bitcast), calls=%async_computation.1 | async-start | bytes 1048576 | tf_op jit(solution)/shard_map/all_to_all | solution.py:26
  28.4 0.7 iota_compare_fusion.2
  29.1 14.2 %all-to-all-done.1 = bf16[32,16,512]{2,1,0:T(8,128)(2,1)S(1)} async-done(((bf16[32,16,512]{2,1,0:T(8,128)(2,1)}), bf16[32,16,512]{2,1,0:T(8,128)(2,1)S(1)}, u32[]{:S(2)}, u32[]{:S(2)}) %all-to-all-start.1) | async-done | bytes 524320 | tf_op jit(solution)/shard_map/all_to_all | solution.py:26
  43.4 3.4 %fusion.32 = (f32[16,2,1024]{2,1,0:T(2,128)S(1)}, f32[16,2,1024]{2,1,0:T(2,128)S(1)}) fusion(pred[16,1024]{1,0:T(8,128)(4,1)S(1)} %iota_compare_fusion.2, f32[2]{0:T(128)} %param.26, bf16[16,2,128]{2,1,0:T(2,128)(2,1)S(1)} %reshape.237, bf16[16,1024,1,128]{3,1,2,0:T(8,128)(2,1)} %param.27), kind=kOutput, calls=%fused_computation.44 | convolution fusion | flops 8716288 | bytes 4481032 | tf_op jit(solution)/shard_map/skgd,slkd->skgl/dot_general | solution.py:129
  47.0 39.6 %reduce-window.14 = f32[16,1,2,8,128]{4,3,2,1,0:T(8,128)S(1)} reduce-window(f32[16,1,2,8,128]{4,3,2,1,0:T(8,128)S(1)} %bitcast.111, f32[]{:T(128)} %constant.52.clone.1), window={size=1x1x1x1x128 pad=0_0x0_0x0_0x0_0x0_127}, to_apply=%region_3.4 | reduce-window | flops 4161536 | bytes 262148 | tf_op jit(solution)/shard_map/reduce-window
  86.6 0.2 copy.77
  87.1 3.3 %multiply_reduce_fusion.1 = (f32[16,2]{1,0:T(8,128)S(1)}, f32[16,2,128]{2,1,0:T(2,128)S(1)}) fusion(bf16[16,1024,1,128]{3,1,2,0:T(8,128)(2,1)} %param.28, pred[16,1024]{1,0:T(8,128)(4,1)S(1)} %iota_compare_fusion.2, f32[16,2,1024]{2,1,0:T(2,128)S(1)} %reshape.240, f32[16,2,1024]{2,1,0:T(2,128)S(1)} %reshape.243, f32[16,2,1024]{2,1,0:T(2,128)S(1)} %get-tuple-element.6), kind=kOutput, calls=%fused_computation.75 | convolution fusion | flops 9084896 | bytes 4620416 | tf_op jit(solution)/shard_map/skgl,slkd->skgd/dot_general | solution.py:141
  90.6 0.7 broadcast_in_dim.39
  91.3 6.3 %all-to-all-start.2 = ((bf16[32,16,256]{2,1,0:T(8,128)(2,1)}), bf16[32,16,256]{2,1,0:T(8,128)(2,1)S(1)}, u32[]{:S(2)}, u32[]{:S(2)}) async-start(bf16[32,16,256]{2,1,0:T(8,128)(2,1)} %broadcast_in_dim.39), calls=%async_computation.2 | async-start | bytes 524288 | tf_op jit(solution)/shard_map/all_to_all | solution.py:11
  97.6 0.1 copy.81
  97.8 0.2 eq.29
  98.0 10.1 %all-to-all-done.2 = bf16[32,16,256]{2,1,0:T(8,128)(2,1)S(1)} async-done(((bf16[32,16,256]{2,1,0:T(8,128)(2,1)}), bf16[32,16,256]{2,1,0:T(8,128)(2,1)S(1)}, u32[]{:S(2)}, u32[]{:S(2)}) %all-to-all-start.2) | async-done | bytes 262176 | tf_op jit(solution)/shard_map/all_to_all | solution.py:11
  108.0 0.2 convolution_convert_fusion.4
  108.3 1.1 broadcast_in_dim.40
  109.4 8.2 %all-to-all-start.3 = ((bf16[8,512,128]{2,1,0:T(8,128)(2,1)}), bf16[8,512,128]{2,1,0:T(8,128)(2,1)S(1)}, u32[]{:S(2)}, u32[]{:S(2)}) async-start(bf16[8,512,128]{2,1,0:T(8,128)(2,1)} %broadcast_in_dim.40), calls=%async_computation.3 | async-start | bytes 2097152 | tf_op jit(solution)/shard_map/all_to_all | solution.py:11
  117.6 0.2 eq.25
  117.8 9.0 %reduce-window.16 = s32[32,8,128]{2,1,0:T(8,128)S(1)} reduce-window(s32[32,8,128]{2,1,0:T(8,128)S(1)} %fusion.43, s32[]{:T(128)} %constant.60.clone.1), window={size=1x1x128 pad=0_0x0_0x127_0}, to_apply=%region_9.10 | reduce-window | flops 4161536 | bytes 262148 | tf_op jit(solution)/shard_map/reduce-window.2
  127.1 0.2 copy.80
  127.3 0.2 mul.143
  127.7 4.3 %scatter_custom_fusion = s32[2048]{0:T(1024)S(1)} fusion(s32[1024]{0:T(1024)S(1)} %bitcast.121, s32[1024]{0:T(1024)S(1)} %add_select_fusion, s32[]{:T(128)} %constant.58.clone.1), kind=kCustom, calls=%fused_computation.86 | custom fusion | bytes 8196 | tf_op jit(solution)/shard_map/scatter | solution.py:81
  132.0 0.6 all-to-all-done.3
  132.6 0.1 reduce_sum.134
  132.7 0.1 multiply_reduce_fusion
  132.9 0.7 broadcast_in_dim.41
  133.6 3.9 %all-to-all-start.4 = ((f32[32,1,512]{2,1,0:T(1,128)}), f32[32,1,512]{2,1,0:T(1,128)S(1)}, u32[]{:S(2)}, u32[]{:S(2)}) async-start(f32[32,1,512]{2,1,0:T(1,128)} %broadcast_in_dim.41), calls=%async_computation.4 | async-start | bytes 131072 | tf_op jit(solution)/shard_map/all_to_all | solution.py:11
  137.4 8.9 %all-to-all-done.4 = f32[32,1,512]{2,1,0:T(1,128)S(1)} async-done(((f32[32,1,512]{2,1,0:T(1,128)}), f32[32,1,512]{2,1,0:T(1,128)S(1)}, u32[]{:S(2)}, u32[]{:S(2)}) %all-to-all-start.4) | async-done | bytes 65568 | tf_op jit(solution)/shard_map/all_to_all | solution.py:11
  146.5 6.2 %gather_fusion = bf16[2048,128]{1,0:T(8,128)(2,1)S(1)} fusion(bf16[513,128]{1,0:T(8,128)(2,1)S(1)} %concatenate.10, s32[2048]{0:T(1024)S(1)} %fusion.52), kind=kCustom, calls=%fused_computation | custom fusion | bytes 1056768 | tf_op jit(solution)/shard_map/gather | solution.py:162
  152.8 12.0 %all_to_all.86 = bf16[32,8,128]{2,1,0:T(8,128)(2,1)S(1)} all-to-all(bf16[32,8,128]{2,1,0:T(8,128)(2,1)S(1)} %constant_dynamic-slice_fusion), channel_id=1, replica_groups=mesh['ep'=32,'tp'=8] {'ep'}, dimensions={0} | all-to-all | bytes 131072 | tf_op jit(solution)/shard_map/all_to_all | solution.py:165
  164.8 16.2 %all_gather.3 = bf16[1,64,4096]{2,1,0:T(8,128)(2,1)S(1)} all-gather(bf16[1,8,4096]{2,1,0:T(8,128)(2,1)S(1)} %bitcast.112), channel_id=1, replica_groups=mesh['ep'=32,'tp'=8] {'tp'}, dimensions={1}, use_global_device_ids=true | all-gather | bytes 589824 | tf_op jit(solution)/shard_map/all_gather | solution.py:166
  181.0 1.5 fusion.15
  182.5 1.4 fusion
  183.9 3.6 %all-to-all-start.6 = ((bf16[8,1,8,4096]{3,2,1,0:T(8,128)(2,1)}), bf16[8,1,8,4096]{3,2,1,0:T(8,128)(2,1)S(1)}, u32[]{:S(2)}, u32[]{:S(2)}) async-start(bf16[8,1,8,4096]{3,2,1,0:T(8,128)(2,1)} %fusion), calls=%async_computation.6 | async-start | bytes 1048576 | tf_op jit(solution)/shard_map/all_to_all | solution.py:26
  187.5 1.4 convolution_convert_fusion.1
  188.9 8.0 %all-to-all-done.6 = bf16[8,1,8,4096]{3,2,1,0:T(8,128)(2,1)S(1)} async-done(((bf16[8,1,8,4096]{3,2,1,0:T(8,128)(2,1)}), bf16[8,1,8,4096]{3,2,1,0:T(8,128)(2,1)S(1)}, u32[]{:S(2)}, u32[]{:S(2)}) %all-to-all-start.6) | async-done | bytes 524320 | tf_op jit(solution)/shard_map/all_to_all | solution.py:26
  196.9 4.8 %all-to-all-start.9 = ((bf16[32,16,1024]{2,1,0:T(8,128)(2,1)}), bf16[32,16,1024]{2,1,0:T(8,128)(2,1)}, u32[]{:S(2)}, u32[]{:S(2)}) async-start(bf16[32,16,1024]{2,1,0:T(8,128)(2,1)} %bitcast.28), calls=%async_computation.9 | async-start | bytes 2097152 | tf_op jit(solution)/shard_map/all_to_all | solution.py:26
  201.8 2.8 copy.86
  204.6 0.5 broadcast.165
  205.1 23.4 %reduce.9 = bf16[4096,8]{1,0:T(8,128)(2,1)} reduce(bf16[4096,1,8]{2,1,0:T(2,128)(2,1)S(1)} %bitcast.103, bf16[]{:T(256)} %broadcast.165), dimensions={1}, to_apply=%bitcast.86.reduce_sub_computation | reduce | bytes 131074
  228.5 3.1 reshape.282
  231.6 9.1 %all-to-all-start.7 = ((bf16[32,2,512]{2,1,0:T(2,128)(2,1)}), bf16[32,2,512]{2,1,0:T(2,128)(2,1)S(1)}, u32[]{:S(2)}, u32[]{:S(2)}) async-start(bf16[32,2,512]{2,1,0:T(2,128)(2,1)} %reshape.282), calls=%async_computation.7 | async-start | bytes 131072 | tf_op jit(solution)/shard_map/all_to_all | solution.py:169
  240.8 1.4 convert_reduce_fusion
  242.2 7.4 %all-to-all-done.7 = bf16[32,2,512]{2,1,0:T(2,128)(2,1)S(1)} async-done(((bf16[32,2,512]{2,1,0:T(2,128)(2,1)}), bf16[32,2,512]{2,1,0:T(2,128)(2,1)S(1)}, u32[]{:S(2)}, u32[]{:S(2)}) %all-to-all-start.7) | async-done | bytes 65568 | tf_op jit(solution)/shard_map/all_to_all | solution.py:169
  249.6 0.9 broadcast_in_dim.46
  250.4 4.6 %all-to-all-start.10 = ((bf16[32,16,512]{2,1,0:T(8,128)(2,1)}), bf16[32,16,512]{2,1,0:T(8,128)(2,1)}, u32[]{:S(2)}, u32[]{:S(2)}) async-start(bf16[32,16,512]{2,1,0:T(8,128)(2,1)} %broadcast_in_dim.46), calls=%async_computation.10 | async-start | bytes 1048576 | tf_op jit(solution)/shard_map/all_to_all | solution.py:11
  255.1 2.8 reshape.283
  257.9 1.9 copy.87
  259.8 9.4 %all-to-all-done.10 = bf16[32,16,512]{2,1,0:T(8,128)(2,1)} async-done(((bf16[32,16,512]{2,1,0:T(8,128)(2,1)}), bf16[32,16,512]{2,1,0:T(8,128)(2,1)}, u32[]{:S(2)}, u32[]{:S(2)}) %all-to-all-start.10) | async-done | bytes 524320 | tf_op jit(solution)/shard_map/all_to_all | solution.py:11
  269.2 0.9 broadcast_in_dim.45
  270.1 8.2 %all-to-all-start.8 = ((bf16[8,32,8,128]{3,2,1,0:T(8,128)(2,1)}), bf16[8,32,8,128]{3,2,1,0:T(8,128)(2,1)S(1)}, u32[]{:S(2)}, u32[]{:S(2)}) async-start(bf16[8,32,8,128]{3,2,1,0:T(8,128)(2,1)} %broadcast_in_dim.45), calls=%async_computation.8 | async-start | bytes 1048576 | tf_op jit(solution)/shard_map/all_to_all | solution.py:11
  278.3 1.3 convolution_convert_fusion.3
  279.6 8.0 %all-to-all-done.8 = bf16[8,32,8,128]{3,2,1,0:T(8,128)(2,1)S(1)} async-done(((bf16[8,32,8,128]{3,2,1,0:T(8,128)(2,1)}), bf16[8,32,8,128]{3,2,1,0:T(8,128)(2,1)S(1)}, u32[]{:S(2)}, u32[]{:S(2)}) %all-to-all-start.8) | async-done | bytes 524320 | tf_op jit(solution)/shard_map/all_to_all | solution.py:11
  287.7 1.1 broadcast_in_dim.47
  288.8 4.4 %all-to-all-start.11 = ((bf16[8,512,128]{2,1,0:T(8,128)(2,1)}), bf16[8,512,128]{2,1,0:T(8,128)(2,1)S(1)}, u32[]{:S(2)}, u32[]{:S(2)}) async-start(bf16[8,512,128]{2,1,0:T(8,128)(2,1)} %broadcast_in_dim.47), calls=%async_computation.11 | async-start | bytes 2097152 | tf_op jit(solution)/shard_map/all_to_all | solution.py:11
  293.2 0.9 copy.90
  294.1 0.6 fusion.63
  294.7 0.1 copy.89
  294.9 3.2 %gather_fusion.1 = bf16[1024,128]{1,0:T(8,128)(2,1)S(1)} fusion(bf16[2048,128]{1,0:T(8,128)(2,1)S(1)} %bitcast.102, s32[1024]{0:T(1024)S(1)} %broadcast_clamp_fusion), kind=kCustom, calls=%fused_computation.1 | custom fusion | bytes 528384 | tf_op jit(solution)/shard_map/gather | solution.py:171
  298.1 3.7 %fusion.17 = f32[512,128]{1,0:T(8,128)S(1)} fusion(bf16[512,2,128]{2,1,0:T(2,128)(2,1)S(1)} %bitcast.107, f32[512,2]{1,0:T(8,128)} %copy.90), kind=kLoop, calls=%fused_computation.23 | loop fusion | flops 327680 | bytes 528384 | tf_op jit(solution)/shard_map/reduce_sum | solution.py:176
  301.8 6.4 %all-to-all-done.11 = bf16[8,512,128]{2,1,0:T(8,128)(2,1)S(1)} async-done(((bf16[8,512,128]{2,1,0:T(8,128)(2,1)}), bf16[8,512,128]{2,1,0:T(8,128)(2,1)S(1)}, u32[]{:S(2)}, u32[]{:S(2)}) %all-to-all-start.11) | async-done | bytes 1048608 | tf_op jit(solution)/shard_map/all_to_all | solution.py:11
  308.2 0.1 reduce_sum.144
  308.4 0.7 add_convert_fusion
  (63 shorter events, 1.8 us)
Async XLA Ops:
  0.6 181.9 %copy-start = (bf16[1,128,4096]{2,1,0:T(8,128)(2,1)S(1)}, bf16[1,128,4096]{2,1,0:T(8,128)(2,1)}, u32[]{:S(2)}) copy-start(bf16[1,128,4096]{2,1,0:T(8,128)(2,1)} %param.37) | copy-start | bytes 3145732
  24.5 18.8 %all-to-all-start.1 = ((bf16[32,16,512]{2,1,0:T(8,128)(2,1)}), bf16[32,16,512]{2,1,0:T(8,128)(2,1)S(1)}, u32[]{:S(2)}, u32[]{:S(2)}) async-start(bf16[32,16,512]{2,1,0:T(8,128)(2,1)} %bitcast), calls=%async_computation.1 | async-start | bytes 1048576 | tf_op jit(solution)/shard_map/all_to_all | solution.py:26
  46.8 43.6 %copy-start.8 = (f32[256]{0:T(256)S(1)}, f32[256]{0:T(256)}, u32[]{:S(2)}) copy-start(f32[256]{0:T(256)} %param.31) | copy-start | bytes 3076
  46.8 50.8 %copy-start.6 = (s32[512,2]{0,1:T(2,128)S(1)}, s32[512,2]{0,1:T(2,128)}, u32[]{:S(2)}) copy-start(s32[512,2]{0,1:T(2,128)} %param.33) | copy-start | bytes 12292
  46.9 61.1 %copy-start.5 = (bf16[256,128]{1,0:T(8,128)(2,1)S(1)}, bf16[256,128]{1,0:T(8,128)(2,1)}, u32[]{:S(2)}) copy-start(bf16[256,128]{1,0:T(8,128)(2,1)} %param.30) | copy-start | bytes 196612
  90.5 42.2 %copy-start.1 = (bf16[512,128]{1,0:T(8,128)(2,1)S(1)}, bf16[512,128]{1,0:T(8,128)(2,1)}, u32[]{:S(2)}) copy-start(bf16[512,128]{1,0:T(8,128)(2,1)} %param.21) | copy-start | bytes 393220
  91.3 55.1 %copy-start.9 = (f32[128]{0:T(128)S(1)}, f32[128]{0:T(128)}, u32[]{:S(2)}) copy-start(f32[128]{0:T(128)} %param.32) | copy-start | bytes 1540
  91.3 16.7 %all-to-all-start.2 = ((bf16[32,16,256]{2,1,0:T(8,128)(2,1)}), bf16[32,16,256]{2,1,0:T(8,128)(2,1)S(1)}, u32[]{:S(2)}, u32[]{:S(2)}) async-start(bf16[32,16,256]{2,1,0:T(8,128)(2,1)} %broadcast_in_dim.39), calls=%async_computation.2 | async-start | bytes 524288 | tf_op jit(solution)/shard_map/all_to_all | solution.py:11
  109.4 23.2 %all-to-all-start.3 = ((bf16[8,512,128]{2,1,0:T(8,128)(2,1)}), bf16[8,512,128]{2,1,0:T(8,128)(2,1)S(1)}, u32[]{:S(2)}, u32[]{:S(2)}) async-start(bf16[8,512,128]{2,1,0:T(8,128)(2,1)} %broadcast_in_dim.40), calls=%async_computation.3 | async-start | bytes 2097152 | tf_op jit(solution)/shard_map/all_to_all | solution.py:11
  132.7 49.8 %copy-start.2 = (bf16[1,4096,128]{2,1,0:T(8,128)(2,1)S(1)}, bf16[1,4096,128]{2,1,0:T(8,128)(2,1)}, u32[]{:S(2)}) copy-start(bf16[1,4096,128]{2,1,0:T(8,128)(2,1)} %param.36) | copy-start | bytes 3145732
  133.6 12.7 %all-to-all-start.4 = ((f32[32,1,512]{2,1,0:T(1,128)}), f32[32,1,512]{2,1,0:T(1,128)S(1)}, u32[]{:S(2)}, u32[]{:S(2)}) async-start(f32[32,1,512]{2,1,0:T(1,128)} %broadcast_in_dim.41), calls=%async_computation.4 | async-start | bytes 131072 | tf_op jit(solution)/shard_map/all_to_all | solution.py:11
  152.7 34.8 %copy-start.3 = (bf16[128,512]{1,0:T(8,128)(2,1)S(1)}, bf16[128,512]{1,0:T(8,128)(2,1)}, u32[]{:S(2)}) copy-start(bf16[128,512]{1,0:T(8,128)(2,1)} %param.39) | copy-start | bytes 393220
  152.7 34.8 %copy-start.4 = (bf16[128,512]{1,0:T(8,128)(2,1)S(1)}, bf16[128,512]{1,0:T(8,128)(2,1)}, u32[]{:S(2)}) copy-start(bf16[128,512]{1,0:T(8,128)(2,1)} %param.38) | copy-start | bytes 393220
  183.9 12.9 %all-to-all-start.6 = ((bf16[8,1,8,4096]{3,2,1,0:T(8,128)(2,1)}), bf16[8,1,8,4096]{3,2,1,0:T(8,128)(2,1)S(1)}, u32[]{:S(2)}, u32[]{:S(2)}) async-start(bf16[8,1,8,4096]{3,2,1,0:T(8,128)(2,1)} %fusion), calls=%async_computation.6 | async-start | bytes 1048576 | tf_op jit(solution)/shard_map/all_to_all | solution.py:26
  196.9 34.7 %all-to-all-start.9 = ((bf16[32,16,1024]{2,1,0:T(8,128)(2,1)}), bf16[32,16,1024]{2,1,0:T(8,128)(2,1)}, u32[]{:S(2)}, u32[]{:S(2)}) async-start(bf16[32,16,1024]{2,1,0:T(8,128)(2,1)} %bitcast.28), calls=%async_computation.9 | async-start | bytes 2097152 | tf_op jit(solution)/shard_map/all_to_all | solution.py:26
  231.6 18.0 %all-to-all-start.7 = ((bf16[32,2,512]{2,1,0:T(2,128)(2,1)}), bf16[32,2,512]{2,1,0:T(2,128)(2,1)S(1)}, u32[]{:S(2)}, u32[]{:S(2)}) async-start(bf16[32,2,512]{2,1,0:T(2,128)(2,1)} %reshape.282), calls=%async_computation.7 | async-start | bytes 131072 | tf_op jit(solution)/shard_map/all_to_all | solution.py:169
  250.4 18.8 %all-to-all-start.10 = ((bf16[32,16,512]{2,1,0:T(8,128)(2,1)}), bf16[32,16,512]{2,1,0:T(8,128)(2,1)}, u32[]{:S(2)}, u32[]{:S(2)}) async-start(bf16[32,16,512]{2,1,0:T(8,128)(2,1)} %broadcast_in_dim.46), calls=%async_computation.10 | async-start | bytes 1048576 | tf_op jit(solution)/shard_map/all_to_all | solution.py:11
  257.9 35.4 %copy-start.7 = (f32[512,2]{0,1:T(2,128)S(1)}, f32[512,2]{0,1:T(2,128)}, u32[]{:S(2)}) copy-start(f32[512,2]{0,1:T(2,128)} %param.34) | copy-start | bytes 12292
  270.1 17.6 %all-to-all-start.8 = ((bf16[8,32,8,128]{3,2,1,0:T(8,128)(2,1)}), bf16[8,32,8,128]{3,2,1,0:T(8,128)(2,1)S(1)}, u32[]{:S(2)}, u32[]{:S(2)}) async-start(bf16[8,32,8,128]{3,2,1,0:T(8,128)(2,1)} %broadcast_in_dim.45), calls=%async_computation.8 | async-start | bytes 1048576 | tf_op jit(solution)/shard_map/all_to_all | solution.py:11
  279.6 28.7 %copy-start.10 = (f32[128]{0:T(128)S(1)}, f32[128]{0:T(128)}, u32[]{:S(2)}) copy-start(f32[128]{0:T(128)} %param.41) | copy-start | bytes 1540
  288.8 19.4 %all-to-all-start.11 = ((bf16[8,512,128]{2,1,0:T(8,128)(2,1)}), bf16[8,512,128]{2,1,0:T(8,128)(2,1)S(1)}, u32[]{:S(2)}, u32[]{:S(2)}) async-start(bf16[8,512,128]{2,1,0:T(8,128)(2,1)} %broadcast_in_dim.47), calls=%async_computation.11 | async-start | bytes 2097152 | tf_op jit(solution)/shard_map/all_to_all | solution.py:11
where the time goes:
time: 310 us; the launch traced here: 309 us
  other arithmetic  81 us (26%)
  waiting for transfers between devices  72.8 us (23%)
  starting transfers between devices  57.1 us (18%)
  blocking collectives  48.7 us (16%)
  local copies, waits for them, and re-layouts  33.7 us (11%)
  matrix products  14.7 us (5%)
    another operation x5, other arithmetic  48.8 us
    all_to_all x6, waiting for transfers between devices, sent_to_all(): lax.all_to_all(jnp.broadcast_to(x[None], (size, *x.shape)), axis, 0, 0, t...  43.3 us
    all_to_all x6, starting transfers between devices, sent_to_all(): lax.all_to_all(jnp.broadcast_to(x[None], (size, *x.shape)), axis, 0, 0, t...  35.6 us
    unnamed x1, other arithmetic  23.4 us
    all_to_all x3, waiting for transfers between devices, sent_and_summed(): lax.all_to_all(blocks, axis, split_axis=0, concat_axis=0, tiled=True)  22.1 us
    all_to_all x1, blocking collectives, sent_to_all(): lax.all_to_all(jnp.broadcast_to(x[None], (size, *x.shape)), axis, 0, 0, t...  20.5 us
    all_gather x1, blocking collectives, per_device(): gathered = lax.all_gather(arrived, 'tp', axis=1, tiled=True)  16.2 us
    all_to_all x3, starting transfers between devices, sent_and_summed(): lax.all_to_all(blocks, axis, split_axis=0, concat_axis=0, tiled=True)  12.3 us
  transfers between devices with their start and end apart: 10, of which 9 were waited for; matrix products, arithmetic and copies ran while one was open for 20% of the time, Pallas kernels for 0%

commit v1 on v0

--- a/solution.py
+++ b/solution.py
@@ -163,7 +163,30 @@
     slot_share = capacity // lax.axis_size("tp")
     own_slots = lax.dynamic_slice_in_dim(outgoing, lax.axis_index("tp") * slot_share, slot_share, 1)
     arrived = lax.all_to_all(own_slots, "ep", split_axis=0, concat_axis=2, tiled=True)
-    gathered = lax.all_gather(arrived, "tp", axis=1, tiled=True)
+    met_up = lax.axis_size("tp")
+    kept_arr, d_next, top = (met_up, lax.axis_index("tp"), arrived.shape[1])
+    lanes = []
+    for i0, idx in enumerate(arrived.shape):
+        lanes.append(idx * kept_arr if i0 == 1 else idx)
+    carry_in = jnp.zeros(lanes, arrived.dtype)
+    gathered = lax.dynamic_update_slice_in_dim(carry_in, arrived, d_next * top, axis=1)
+    ready = outer = arrived
+    for no in tuple(range(1, kept_arr // 2 + 1)):
+        chunks = []
+        for i0 in tuple(range(kept_arr)):
+            chunks.append((i0, (i0 + 1) % kept_arr))
+        ready = lax.ppermute(ready, axis_name="tp", perm=chunks)
+        gathered = lax.dynamic_update_slice_in_dim(
+            gathered, ready, (d_next - no) % kept_arr * top, axis=1
+        )
+        if 2 * no < kept_arr:
+            in_order = []
+            for i0 in [*range(kept_arr)]:
+                in_order.append((i0, (i0 - 1) % kept_arr))
+            outer = lax.ppermute(outer, axis_name="tp", perm=in_order)
+            gathered = lax.dynamic_update_slice_in_dim(
+                gathered, outer, (d_next + no) % kept_arr * top, axis=1
+            )
     partial_value = expert_terms(gathered, expert_gate, expert_up, expert_down)
     summed = sent_and_summed(partial_value.astype(jnp.bfloat16), "tp", 1).astype(jnp.bfloat16)
     came_back = lax.all_to_all(summed, "ep", split_axis=2, concat_axis=0, tiled=True)

time: 310 us -> 318 us (1.026)
  blocking collectives: 48.7 us -> 20.5 us
  starting transfers between devices: 57.1 us -> 76 us
  waiting for transfers between devices: 72.8 us -> 89 us
    all_gather x1 -> x0, blocking collectives: 16.2 us -> none  [per_device(): gathered = lax.all_gather(arrived, 'tp', axis=1, tiled=True)]
    all_to_all x1 -> x0, blocking collectives: 12 us -> none  [per_device(): lax.all_to_all(own_slots, 'ep', split_axis=0, concat_axis=2, tiled=True)]
    ppermute x0 -> x7, starting transfers between devices: none -> 11.1 us  [the longest x4 8.39 us: per_device(): ready = lax.ppermute(ready, axis_name='tp', perm=chunks)]
    all_to_all x0 -> x1, waiting for transfers between devices: none -> 8.74 us  [per_device(): lax.all_to_all(own_slots, 'ep', split_axis=0, concat_axis=2, tiled=True)]
    ppermute x0 -> x7, waiting for transfers between devices: none -> 7.46 us  [the longest x4 6.59 us: per_device(): ready = lax.ppermute(ready, axis_name='tp', perm=chunks)]
    all_to_all x3, starting transfers between devices: 12.3 us -> 16.3 us  [sent_and_summed(): lax.all_to_all(blocks, axis, split_axis=0, concat_axis=0, tiled=True)]
    all_to_all x0 -> x1, starting transfers between devices: none -> 3.86 us  [per_device(): lax.all_to_all(own_slots, 'ep', split_axis=0, concat_axis=2, tiled=True)]
  transfers between devices with their start and end apart: 10 -> 18, of which waited for: 9 -> 17; matrix products, arithmetic and copies ran while one was open for 20% -> 20% of each run, Pallas kernels for 0% -> 0%
where the time goes in v1:
time: 318 us; the launch traced here: 317 us
  waiting for transfers between devices  89 us (28%)
  other arithmetic  81 us (25%)
  starting transfers between devices  76 us (24%)
  local copies, waits for them, and re-layouts  34.4 us (11%)
  blocking collectives  20.5 us (6%)
  matrix products  14.7 us (5%)
    another operation x5, other arithmetic  48.8 us
    all_to_all x6, waiting for transfers between devices, sent_to_all(): lax.all_to_all(jnp.broadcast_to(x[None], (size, *x.shape)), axis, 0, 0, t...  43.3 us
    all_to_all x6, starting transfers between devices, sent_to_all(): lax.all_to_all(jnp.broadcast_to(x[None], (size, *x.shape)), axis, 0, 0, t...  35.6 us
    unnamed x1, other arithmetic  23.4 us
    all_to_all x3, waiting for transfers between devices, sent_and_summed(): lax.all_to_all(blocks, axis, split_axis=0, concat_axis=0, tiled=True)  22.1 us
    all_to_all x1, blocking collectives, sent_to_all(): lax.all_to_all(jnp.broadcast_to(x[None], (size, *x.shape)), axis, 0, 0, t...  20.5 us
    all_to_all x3, starting transfers between devices, sent_and_summed(): lax.all_to_all(blocks, axis, split_axis=0, concat_axis=0, tiled=True)  16.3 us
    all_to_all x1, starting transfers between devices, per_device(): lax.all_to_all(summed, 'ep', split_axis=2, concat_axis=0, tiled=True)  9.14 us
  transfers between devices with their start and end apart: 18, of which 17 were waited for; matrix products, arithmetic and copies ran while one was open for 20% of the time, Pallas kernels for 0%

profile of v1, /device:TPU:1, one launch (start us, length us, event | category | flops | bytes accessed | tf_op | source)
XLA Modules:
  0.0 317.0 jit_solution(4911465647891334685)
XLA Ops:
  0.6 1.1 fusion.17
  1.8 20.5 %all_to_all.85 = f32[32,1,512]{2,1,0:T(1,128)S(1)} all-to-all(f32[32,1,512]{2,1,0:T(1,128)S(1)} %broadcast_in_dim.37), channel_id=1, replica_groups=mesh['ep'=32,'tp'=8] {'ep'}, dimensions={0} | all-to-all | bytes 131072 | tf_op jit(solution)/shard_map/all_to_all | solution.py:11
  22.4 2.1 convolution_convert_fusion.2
  24.5 3.9 %all-to-all-start.1 = ((bf16[32,16,512]{2,1,0:T(8,128)(2,1)}), bf16[32,16,512]{2,1,0:T(8,128)(2,1)S(1)}, u32[]{:S(2)}, u32[]{:S(2)}) async-start(bf16[32,16,512]{2,1,0:T(8,128)(2,1)} %bitcast), calls=%async_computation.1 | async-start | bytes 1048576 | tf_op jit(solution)/shard_map/all_to_all | solution.py:26
  28.4 0.7 iota_compare_fusion.2
  29.1 14.2 %all-to-all-done.1 = bf16[32,16,512]{2,1,0:T(8,128)(2,1)S(1)} async-done(((bf16[32,16,512]{2,1,0:T(8,128)(2,1)}), bf16[32,16,512]{2,1,0:T(8,128)(2,1)S(1)}, u32[]{:S(2)}, u32[]{:S(2)}) %all-to-all-start.1) | async-done | bytes 524320 | tf_op jit(solution)/shard_map/all_to_all | solution.py:26
  43.4 3.4 %fusion.28 = (f32[16,2,1024]{2,1,0:T(2,128)S(1)}, f32[16,2,1024]{2,1,0:T(2,128)S(1)}) fusion(pred[16,1024]{1,0:T(8,128)(4,1)S(1)} %iota_compare_fusion.2, f32[2]{0:T(128)} %param.26, bf16[16,2,128]{2,1,0:T(2,128)(2,1)S(1)} %reshape.268, bf16[16,1024,1,128]{3,1,2,0:T(8,128)(2,1)} %param.27), kind=kOutput, calls=%fused_computation.41 | convolution fusion | flops 8716288 | bytes 4481032 | tf_op jit(solution)/shard_map/skgd,slkd->skgl/dot_general | solution.py:129
  47.0 39.6 %reduce-window.14 = f32[16,1,2,8,128]{4,3,2,1,0:T(8,128)S(1)} reduce-window(f32[16,1,2,8,128]{4,3,2,1,0:T(8,128)S(1)} %bitcast.127, f32[]{:T(128)} %constant.101.clone.1), window={size=1x1x1x1x128 pad=0_0x0_0x0_0x0_0x0_127}, to_apply=%region_3.4 | reduce-window | flops 4161536 | bytes 262148 | tf_op jit(solution)/shard_map/reduce-window
  87.1 3.3 %multiply_reduce_fusion.1 = (f32[16,2]{1,0:T(8,128)S(1)}, f32[16,2,128]{2,1,0:T(2,128)S(1)}) fusion(bf16[16,1024,1,128]{3,1,2,0:T(8,128)(2,1)} %param.28, pred[16,1024]{1,0:T(8,128)(4,1)S(1)} %iota_compare_fusion.2, f32[16,2,1024]{2,1,0:T(2,128)S(1)} %reshape.271, f32[16,2,1024]{2,1,0:T(2,128)S(1)} %reshape.274, f32[16,2,1024]{2,1,0:T(2,128)S(1)} %get-tuple-element.6), kind=kOutput, calls=%fused_computation.76 | convolution fusion | flops 9084896 | bytes 4620416 | tf_op jit(solution)/shard_map/skgl,slkd->skgd/dot_general | solution.py:141
  90.6 0.7 broadcast_in_dim.39
  91.3 6.3 %all-to-all-start.2 = ((bf16[32,16,256]{2,1,0:T(8,128)(2,1)}), bf16[32,16,256]{2,1,0:T(8,128)(2,1)S(1)}, u32[]{:S(2)}, u32[]{:S(2)}) async-start(bf16[32,16,256]{2,1,0:T(8,128)(2,1)} %broadcast_in_dim.39), calls=%async_computation.2 | async-start | bytes 524288 | tf_op jit(solution)/shard_map/all_to_all | solution.py:11
  98.0 10.1 %all-to-all-done.2 = bf16[32,16,256]{2,1,0:T(8,128)(2,1)S(1)} async-done(((bf16[32,16,256]{2,1,0:T(8,128)(2,1)}), bf16[32,16,256]{2,1,0:T(8,128)(2,1)S(1)}, u32[]{:S(2)}, u32[]{:S(2)}) %all-to-all-start.2) | async-done | bytes 262176 | tf_op jit(solution)/shard_map/all_to_all | solution.py:11
  108.3 1.1 broadcast_in_dim.40
  109.4 8.2 %all-to-all-start.3 = ((bf16[8,512,128]{2,1,0:T(8,128)(2,1)}), bf16[8,512,128]{2,1,0:T(8,128)(2,1)S(1)}, u32[]{:S(2)}, u32[]{:S(2)}) async-start(bf16[8,512,128]{2,1,0:T(8,128)(2,1)} %broadcast_in_dim.40), calls=%async_computation.3 | async-start | bytes 2097152 | tf_op jit(solution)/shard_map/all_to_all | solution.py:11
  117.8 9.0 %reduce-window.16 = s32[32,8,128]{2,1,0:T(8,128)S(1)} reduce-window(s32[32,8,128]{2,1,0:T(8,128)S(1)} %fusion.39, s32[]{:T(128)} %constant.109.clone.1), window={size=1x1x128 pad=0_0x0_0x127_0}, to_apply=%region_9.10 | reduce-window | flops 4161536 | bytes 262148 | tf_op jit(solution)/shard_map/reduce-window.2
  127.7 4.3 %scatter_custom_fusion = s32[2048]{0:T(1024)S(1)} fusion(s32[1024]{0:T(1024)S(1)} %bitcast.138, s32[1024]{0:T(1024)S(1)} %add_select_fusion, s32[]{:T(128)} %constant.107.clone.1), kind=kCustom, calls=%fused_computation.87 | custom fusion | bytes 8196 | tf_op jit(solution)/shard_map/scatter | solution.py:81
  132.0 0.6 all-to-all-done.3
  132.9 0.7 broadcast_in_dim.41
  133.5 3.9 %all-to-all-start.4 = ((f32[32,1,512]{2,1,0:T(1,128)}), f32[32,1,512]{2,1,0:T(1,128)S(1)}, u32[]{:S(2)}, u32[]{:S(2)}) async-start(f32[32,1,512]{2,1,0:T(1,128)} %broadcast_in_dim.41), calls=%async_computation.4 | async-start | bytes 131072 | tf_op jit(solution)/shard_map/all_to_all | solution.py:11
  137.4 8.9 %all-to-all-done.4 = f32[32,1,512]{2,1,0:T(1,128)S(1)} async-done(((f32[32,1,512]{2,1,0:T(1,128)}), f32[32,1,512]{2,1,0:T(1,128)S(1)}, u32[]{:S(2)}, u32[]{:S(2)}) %all-to-all-start.4) | async-done | bytes 65568 | tf_op jit(solution)/shard_map/all_to_all | solution.py:11
  146.5 6.2 %gather_fusion = bf16[2048,128]{1,0:T(8,128)(2,1)S(1)} fusion(bf16[513,128]{1,0:T(8,128)(2,1)S(1)} %concatenate.10, s32[2048]{0:T(1024)S(1)} %fusion.47), kind=kCustom, calls=%fused_computation | custom fusion | bytes 1056768 | tf_op jit(solution)/shard_map/gather | solution.py:162
  152.8 0.7 constant_dynamic-slice_fusion
  153.4 3.9 %all-to-all-start.5 = ((bf16[32,8,128]{2,1,0:T(8,128)(2,1)}), bf16[32,8,128]{2,1,0:T(8,128)(2,1)S(1)}, u32[]{:S(2)}, u32[]{:S(2)}) async-start(bf16[32,8,128]{2,1,0:T(8,128)(2,1)} %constant_dynamic-slice_fusion), calls=%async_computation.5 | async-start | bytes 131072 | tf_op jit(solution)/shard_map/all_to_all | solution.py:165
  157.4 8.7 %all-to-all-done.5 = bf16[32,8,128]{2,1,0:T(8,128)(2,1)S(1)} async-done(((bf16[32,8,128]{2,1,0:T(8,128)(2,1)}), bf16[32,8,128]{2,1,0:T(8,128)(2,1)S(1)}, u32[]{:S(2)}, u32[]{:S(2)}) %all-to-all-start.5) | async-done | bytes 65568 | tf_op jit(solution)/shard_map/all_to_all | solution.py:165
  166.1 3.4 %collective-permute-start = (bf16[1,8,4096]{2,1,0:T(8,128)(2,1)S(1)}, bf16[1,8,4096]{2,1,0:T(8,128)(2,1)S(1)}, u32[]{:S(2)}, u32[]{:S(2)}) collective-permute-start(bf16[1,8,4096]{2,1,0:T(8,128)(2,1)S(1)} %bitcast.129), channel_id=1, source_target_pairs={{0,1},{1,2},{2,3},{3,4},{4,5},{5,6},{6,7},{7,0},{8,9},{9,10},{10,1... | collective-permute-start | bytes 196616 | tf_op jit(solution)/shard_map/ppermute | solution.py:178
  169.7 1.3 collective-permute-done
  170.9 2.4 collective-permute-start.2
  173.6 0.8 collective-permute-start.3
  174.4 0.7 collective-permute-done.2
  175.1 1.9 collective-permute-start.4
  177.3 2.0 collective-permute-start.5
  179.3 0.7 collective-permute-done.4
  180.0 0.7 collective-permute-start.6
  181.0 3.9 %collective-permute-done.6 = bf16[1,8,4096]{2,1,0:T(8,128)(2,1)S(1)} collective-permute-done((bf16[1,8,4096]{2,1,0:T(8,128)(2,1)S(1)}, bf16[1,8,4096]{2,1,0:T(8,128)(2,1)S(1)}, u32[]{:S(2)}, u32[]{:S(2)}) %collective-permute-start.6) | collective-permute-done | bytes 65568 | tf_op jit(solution)/shard_map/ppermute | solution.py:178
  184.9 1.5 fusion.12
  186.4 1.4 fusion
  187.9 7.5 %all-to-all-start.6 = ((bf16[8,1,8,4096]{3,2,1,0:T(8,128)(2,1)}), bf16[8,1,8,4096]{3,2,1,0:T(8,128)(2,1)S(1)}, u32[]{:S(2)}, u32[]{:S(2)}) async-start(bf16[8,1,8,4096]{3,2,1,0:T(8,128)(2,1)} %fusion), calls=%async_computation.6 | async-start | bytes 1048576 | tf_op jit(solution)/shard_map/all_to_all | solution.py:26
  195.4 1.4 convolution_convert_fusion.1
  196.8 8.0 %all-to-all-done.6 = bf16[8,1,8,4096]{3,2,1,0:T(8,128)(2,1)S(1)} async-done(((bf16[8,1,8,4096]{3,2,1,0:T(8,128)(2,1)}), bf16[8,1,8,4096]{3,2,1,0:T(8,128)(2,1)S(1)}, u32[]{:S(2)}, u32[]{:S(2)}) %all-to-all-start.6) | async-done | bytes 524320 | tf_op jit(solution)/shard_map/all_to_all | solution.py:26
  204.8 4.8 %all-to-all-start.9 = ((bf16[32,16,1024]{2,1,0:T(8,128)(2,1)}), bf16[32,16,1024]{2,1,0:T(8,128)(2,1)}, u32[]{:S(2)}, u32[]{:S(2)}) async-start(bf16[32,16,1024]{2,1,0:T(8,128)(2,1)} %bitcast.37), calls=%async_computation.9 | async-start | bytes 2097152 | tf_op jit(solution)/shard_map/all_to_all | solution.py:26
  209.7 2.8 copy.86
  212.5 0.5 broadcast.181
  213.0 23.4 %reduce.9 = bf16[4096,8]{1,0:T(8,128)(2,1)} reduce(bf16[4096,1,8]{2,1,0:T(2,128)(2,1)S(1)} %bitcast.119, bf16[]{:T(256)} %broadcast.181), dimensions={1}, to_apply=%bitcast.100.reduce_sub_computation | reduce | bytes 131074
  236.4 3.1 reshape.320
  239.5 9.1 %all-to-all-start.7 = ((bf16[32,2,512]{2,1,0:T(2,128)(2,1)}), bf16[32,2,512]{2,1,0:T(2,128)(2,1)S(1)}, u32[]{:S(2)}, u32[]{:S(2)}) async-start(bf16[32,2,512]{2,1,0:T(2,128)(2,1)} %reshape.320), calls=%async_computation.7 | async-start | bytes 131072 | tf_op jit(solution)/shard_map/all_to_all | solution.py:192
  248.7 1.4 convert_reduce_fusion
  250.1 7.4 %all-to-all-done.7 = bf16[32,2,512]{2,1,0:T(2,128)(2,1)S(1)} async-done(((bf16[32,2,512]{2,1,0:T(2,128)(2,1)}), bf16[32,2,512]{2,1,0:T(2,128)(2,1)S(1)}, u32[]{:S(2)}, u32[]{:S(2)}) %all-to-all-start.7) | async-done | bytes 65568 | tf_op jit(solution)/shard_map/all_to_all | solution.py:192
  257.5 0.9 broadcast_in_dim.46
  258.4 4.6 %all-to-all-start.10 = ((bf16[32,16,512]{2,1,0:T(8,128)(2,1)}), bf16[32,16,512]{2,1,0:T(8,128)(2,1)}, u32[]{:S(2)}, u32[]{:S(2)}) async-start(bf16[32,16,512]{2,1,0:T(8,128)(2,1)} %broadcast_in_dim.46), calls=%async_computation.10 | async-start | bytes 1048576 | tf_op jit(solution)/shard_map/all_to_all | solution.py:11
  263.0 2.8 reshape.321
  265.8 1.9 copy.87
  267.7 9.4 %all-to-all-done.10 = bf16[32,16,512]{2,1,0:T(8,128)(2,1)} async-done(((bf16[32,16,512]{2,1,0:T(8,128)(2,1)}), bf16[32,16,512]{2,1,0:T(8,128)(2,1)}, u32[]{:S(2)}, u32[]{:S(2)}) %all-to-all-start.10) | async-done | bytes 524320 | tf_op jit(solution)/shard_map/all_to_all | solution.py:11
  277.1 0.9 broadcast_in_dim.45
  278.0 8.2 %all-to-all-start.8 = ((bf16[8,32,8,128]{3,2,1,0:T(8,128)(2,1)}), bf16[8,32,8,128]{3,2,1,0:T(8,128)(2,1)S(1)}, u32[]{:S(2)}, u32[]{:S(2)}) async-start(bf16[8,32,8,128]{3,2,1,0:T(8,128)(2,1)} %broadcast_in_dim.45), calls=%async_computation.8 | async-start | bytes 1048576 | tf_op jit(solution)/shard_map/all_to_all | solution.py:11
  286.2 1.3 convolution_convert_fusion.3
  287.6 8.0 %all-to-all-done.8 = bf16[8,32,8,128]{3,2,1,0:T(8,128)(2,1)S(1)} async-done(((bf16[8,32,8,128]{3,2,1,0:T(8,128)(2,1)}), bf16[8,32,8,128]{3,2,1,0:T(8,128)(2,1)S(1)}, u32[]{:S(2)}, u32[]{:S(2)}) %all-to-all-start.8) | async-done | bytes 524320 | tf_op jit(solution)/shard_map/all_to_all | solution.py:11
  295.6 1.1 broadcast_in_dim.47
  296.7 4.4 %all-to-all-start.11 = ((bf16[8,512,128]{2,1,0:T(8,128)(2,1)}), bf16[8,512,128]{2,1,0:T(8,128)(2,1)S(1)}, u32[]{:S(2)}, u32[]{:S(2)}) async-start(bf16[8,512,128]{2,1,0:T(8,128)(2,1)} %broadcast_in_dim.47), calls=%async_computation.11 | async-start | bytes 2097152 | tf_op jit(solution)/shard_map/all_to_all | solution.py:11
  301.2 0.9 copy.90
  302.1 0.6 fusion.58
  302.8 3.2 %gather_fusion.1 = bf16[1024,128]{1,0:T(8,128)(2,1)S(1)} fusion(bf16[2048,128]{1,0:T(8,128)(2,1)S(1)} %bitcast.118, s32[1024]{0:T(1024)S(1)} %broadcast_clamp_fusion), kind=kCustom, calls=%fused_computation.1 | custom fusion | bytes 528384 | tf_op jit(solution)/shard_map/gather | solution.py:194
  306.0 3.7 %fusion.16 = f32[512,128]{1,0:T(8,128)S(1)} fusion(bf16[512,2,128]{2,1,0:T(2,128)(2,1)S(1)} %bitcast.123, f32[512,2]{1,0:T(8,128)} %copy.90), kind=kLoop, calls=%fused_computation.22 | loop fusion | flops 327680 | bytes 528384 | tf_op jit(solution)/shard_map/reduce_sum | solution.py:199
  309.7 6.4 %all-to-all-done.11 = bf16[8,512,128]{2,1,0:T(8,128)(2,1)S(1)} async-done(((bf16[8,512,128]{2,1,0:T(8,128)(2,1)}), bf16[8,512,128]{2,1,0:T(8,128)(2,1)S(1)}, u32[]{:S(2)}, u32[]{:S(2)}) %all-to-all-start.11) | async-done | bytes 1048608 | tf_op jit(solution)/shard_map/all_to_all | solution.py:11
  316.3 0.7 add_convert_fusion
  (86 shorter events, 4.5 us)
Async XLA Ops:
  0.6 185.8 %copy-start = (bf16[1,128,4096]{2,1,0:T(8,128)(2,1)S(1)}, bf16[1,128,4096]{2,1,0:T(8,128)(2,1)}, u32[]{:S(2)}) copy-start(bf16[1,128,4096]{2,1,0:T(8,128)(2,1)} %param.37) | copy-start | bytes 3145732
  24.5 18.8 %all-to-all-start.1 = ((bf16[32,16,512]{2,1,0:T(8,128)(2,1)}), bf16[32,16,512]{2,1,0:T(8,128)(2,1)S(1)}, u32[]{:S(2)}, u32[]{:S(2)}) async-start(bf16[32,16,512]{2,1,0:T(8,128)(2,1)} %bitcast), calls=%async_computation.1 | async-start | bytes 1048576 | tf_op jit(solution)/shard_map/all_to_all | solution.py:26
  46.8 43.6 %copy-start.8 = (f32[256]{0:T(256)S(1)}, f32[256]{0:T(256)}, u32[]{:S(2)}) copy-start(f32[256]{0:T(256)} %param.31) | copy-start | bytes 3076
  46.8 50.8 %copy-start.6 = (s32[512,2]{0,1:T(2,128)S(1)}, s32[512,2]{0,1:T(2,128)}, u32[]{:S(2)}) copy-start(s32[512,2]{0,1:T(2,128)} %param.33) | copy-start | bytes 12292
  46.9 61.1 %copy-start.5 = (bf16[256,128]{1,0:T(8,128)(2,1)S(1)}, bf16[256,128]{1,0:T(8,128)(2,1)}, u32[]{:S(2)}) copy-start(bf16[256,128]{1,0:T(8,128)(2,1)} %param.30) | copy-start | bytes 196612
  90.5 42.2 %copy-start.1 = (bf16[512,128]{1,0:T(8,128)(2,1)S(1)}, bf16[512,128]{1,0:T(8,128)(2,1)}, u32[]{:S(2)}) copy-start(bf16[512,128]{1,0:T(8,128)(2,1)} %param.21) | copy-start | bytes 393220
  91.3 55.1 %copy-start.9 = (f32[128]{0:T(128)S(1)}, f32[128]{0:T(128)}, u32[]{:S(2)}) copy-start(f32[128]{0:T(128)} %param.32) | copy-start | bytes 1540
  91.3 16.7 %all-to-all-start.2 = ((bf16[32,16,256]{2,1,0:T(8,128)(2,1)}), bf16[32,16,256]{2,1,0:T(8,128)(2,1)S(1)}, u32[]{:S(2)}, u32[]{:S(2)}) async-start(bf16[32,16,256]{2,1,0:T(8,128)(2,1)} %broadcast_in_dim.39), calls=%async_computation.2 | async-start | bytes 524288 | tf_op jit(solution)/shard_map/all_to_all | solution.py:11
  109.4 23.2 %all-to-all-start.3 = ((bf16[8,512,128]{2,1,0:T(8,128)(2,1)}), bf16[8,512,128]{2,1,0:T(8,128)(2,1)S(1)}, u32[]{:S(2)}, u32[]{:S(2)}) async-start(bf16[8,512,128]{2,1,0:T(8,128)(2,1)} %broadcast_in_dim.40), calls=%async_computation.3 | async-start | bytes 2097152 | tf_op jit(solution)/shard_map/all_to_all | solution.py:11
  133.5 12.7 %all-to-all-start.4 = ((f32[32,1,512]{2,1,0:T(1,128)}), f32[32,1,512]{2,1,0:T(1,128)S(1)}, u32[]{:S(2)}, u32[]{:S(2)}) async-start(f32[32,1,512]{2,1,0:T(1,128)} %broadcast_in_dim.41), calls=%async_computation.4 | async-start | bytes 131072 | tf_op jit(solution)/shard_map/all_to_all | solution.py:11
  146.5 39.9 %copy-start.2 = (bf16[1,4096,128]{2,1,0:T(8,128)(2,1)S(1)}, bf16[1,4096,128]{2,1,0:T(8,128)(2,1)}, u32[]{:S(2)}) copy-start(bf16[1,4096,128]{2,1,0:T(8,128)(2,1)} %param.35) | copy-start | bytes 3145732
  152.7 42.7 %copy-start.3 = (bf16[128,512]{1,0:T(8,128)(2,1)S(1)}, bf16[128,512]{1,0:T(8,128)(2,1)}, u32[]{:S(2)}) copy-start(bf16[128,512]{1,0:T(8,128)(2,1)} %param.39) | copy-start | bytes 393220
  152.7 42.7 %copy-start.4 = (bf16[128,512]{1,0:T(8,128)(2,1)S(1)}, bf16[128,512]{1,0:T(8,128)(2,1)}, u32[]{:S(2)}) copy-start(bf16[128,512]{1,0:T(8,128)(2,1)} %param.38) | copy-start | bytes 393220
  153.4 12.7 %all-to-all-start.5 = ((bf16[32,8,128]{2,1,0:T(8,128)(2,1)}), bf16[32,8,128]{2,1,0:T(8,128)(2,1)S(1)}, u32[]{:S(2)}, u32[]{:S(2)}) async-start(bf16[32,8,128]{2,1,0:T(8,128)(2,1)} %constant_dynamic-slice_fusion), calls=%async_computation.5 | async-start | bytes 131072 | tf_op jit(solution)/shard_map/all_to_all | solution.py:165
  166.1 4.8 %collective-permute-start = (bf16[1,8,4096]{2,1,0:T(8,128)(2,1)S(1)}, bf16[1,8,4096]{2,1,0:T(8,128)(2,1)S(1)}, u32[]{:S(2)}, u32[]{:S(2)}) collective-permute-start(bf16[1,8,4096]{2,1,0:T(8,128)(2,1)S(1)} %bitcast.129), channel_id=1, source_target_pairs={{0,1},{1,2},{2,3},{3,4},{4,5},{5,6},{6,7},{7,0},{8,9},{9,10},{10,1... | collective-permute-start | bytes 196616 | tf_op jit(solution)/shard_map/ppermute | solution.py:178
  169.6 4.0 %collective-permute-start.1 = (bf16[1,8,4096]{2,1,0:T(8,128)(2,1)S(1)}, bf16[1,8,4096]{2,1,0:T(8,128)(2,1)S(1)}, u32[]{:S(2)}, u32[]{:S(2)}) collective-permute-start(bf16[1,8,4096]{2,1,0:T(8,128)(2,1)S(1)} %bitcast.130), channel_id=1, source_target_pairs={{0,7},{1,0},{2,1},{3,2},{4,3},{5,4},{6,5},{7,6},{8,15},{9,8},{10,9... | collective-permute-start | bytes 196616 | tf_op jit(solution)/shard_map/ppermute | solution.py:186
  170.9 4.1 %collective-permute-start.2 = (bf16[1,8,4096]{2,1,0:T(8,128)(2,1)S(1)}, bf16[1,8,4096]{2,1,0:T(8,128)(2,1)S(1)}, u32[]{:S(2)}, u32[]{:S(2)}) collective-permute-start(bf16[1,8,4096]{2,1,0:T(8,128)(2,1)S(1)} %collective-permute-done), channel_id=1, source_target_pairs={{0,1},{1,2},{2,3},{3,4},{4,5},{5,6},{6,7},{7,0},{8,9},{9,10},{10,1... | collective-permute-start | bytes 196616 | tf_op jit(solution)/shard_map/ppermute | solution.py:178
  173.6 3.7 %collective-permute-start.3 = (bf16[1,8,4096]{2,1,0:T(8,128)(2,1)S(1)}, bf16[1,8,4096]{2,1,0:T(8,128)(2,1)S(1)}, u32[]{:S(2)}, u32[]{:S(2)}) collective-permute-start(bf16[1,8,4096]{2,1,0:T(8,128)(2,1)S(1)} %collective-permute-done.1), channel_id=1, source_target_pairs={{0,7},{1,0},{2,1},{3,2},{4,3},{5,4},{6,5},{7,6},{8,15},{9,8},{10,9... | collective-permute-start | bytes 196616 | tf_op jit(solution)/shard_map/ppermute | solution.py:186
  175.1 4.9 %collective-permute-start.4 = (bf16[1,8,4096]{2,1,0:T(8,128)(2,1)S(1)}, bf16[1,8,4096]{2,1,0:T(8,128)(2,1)S(1)}, u32[]{:S(2)}, u32[]{:S(2)}) collective-permute-start(bf16[1,8,4096]{2,1,0:T(8,128)(2,1)S(1)} %collective-permute-done.2), channel_id=1, source_target_pairs={{0,1},{1,2},{2,3},{3,4},{4,5},{5,6},{6,7},{7,0},{8,9},{9,10},{10,1... | collective-permute-start | bytes 196616 | tf_op jit(solution)/shard_map/ppermute | solution.py:178
  177.3 3.7 %collective-permute-start.5 = (bf16[1,8,4096]{2,1,0:T(8,128)(2,1)S(1)}, bf16[1,8,4096]{2,1,0:T(8,128)(2,1)S(1)}, u32[]{:S(2)}, u32[]{:S(2)}) collective-permute-start(bf16[1,8,4096]{2,1,0:T(8,128)(2,1)S(1)} %collective-permute-done.3), channel_id=1, source_target_pairs={{0,7},{1,0},{2,1},{3,2},{4,3},{5,4},{6,5},{7,6},{8,15},{9,8},{10,9... | collective-permute-start | bytes 196616 | tf_op jit(solution)/shard_map/ppermute | solution.py:186
  180.0 4.9 %collective-permute-start.6 = (bf16[1,8,4096]{2,1,0:T(8,128)(2,1)S(1)}, bf16[1,8,4096]{2,1,0:T(8,128)(2,1)S(1)}, u32[]{:S(2)}, u32[]{:S(2)}) collective-permute-start(bf16[1,8,4096]{2,1,0:T(8,128)(2,1)S(1)} %collective-permute-done.4), channel_id=1, source_target_pairs={{0,1},{1,2},{2,3},{3,4},{4,5},{5,6},{6,7},{7,0},{8,9},{9,10},{10,1... | collective-permute-start | bytes 196616 | tf_op jit(solution)/shard_map/ppermute | solution.py:178
  187.9 16.9 %all-to-all-start.6 = ((bf16[8,1,8,4096]{3,2,1,0:T(8,128)(2,1)}), bf16[8,1,8,4096]{3,2,1,0:T(8,128)(2,1)S(1)}, u32[]{:S(2)}, u32[]{:S(2)}) async-start(bf16[8,1,8,4096]{3,2,1,0:T(8,128)(2,1)} %fusion), calls=%async_computation.6 | async-start | bytes 1048576 | tf_op jit(solution)/shard_map/all_to_all | solution.py:26
  204.8 34.7 %all-to-all-start.9 = ((bf16[32,16,1024]{2,1,0:T(8,128)(2,1)}), bf16[32,16,1024]{2,1,0:T(8,128)(2,1)}, u32[]{:S(2)}, u32[]{:S(2)}) async-start(bf16[32,16,1024]{2,1,0:T(8,128)(2,1)} %bitcast.37), calls=%async_computation.9 | async-start | bytes 2097152 | tf_op jit(solution)/shard_map/all_to_all | solution.py:26
  239.5 18.0 %all-to-all-start.7 = ((bf16[32,2,512]{2,1,0:T(2,128)(2,1)}), bf16[32,2,512]{2,1,0:T(2,128)(2,1)S(1)}, u32[]{:S(2)}, u32[]{:S(2)}) async-start(bf16[32,2,512]{2,1,0:T(2,128)(2,1)} %reshape.320), calls=%async_computation.7 | async-start | bytes 131072 | tf_op jit(solution)/shard_map/all_to_all | solution.py:192
  258.4 18.8 %all-to-all-start.10 = ((bf16[32,16,512]{2,1,0:T(8,128)(2,1)}), bf16[32,16,512]{2,1,0:T(8,128)(2,1)}, u32[]{:S(2)}, u32[]{:S(2)}) async-start(bf16[32,16,512]{2,1,0:T(8,128)(2,1)} %broadcast_in_dim.46), calls=%async_computation.10 | async-start | bytes 1048576 | tf_op jit(solution)/shard_map/all_to_all | solution.py:11
  265.8 35.4 %copy-start.7 = (f32[512,2]{0,1:T(2,128)S(1)}, f32[512,2]{0,1:T(2,128)}, u32[]{:S(2)}) copy-start(f32[512,2]{0,1:T(2,128)} %param.34) | copy-start | bytes 12292
  278.0 17.6 %all-to-all-start.8 = ((bf16[8,32,8,128]{3,2,1,0:T(8,128)(2,1)}), bf16[8,32,8,128]{3,2,1,0:T(8,128)(2,1)S(1)}, u32[]{:S(2)}, u32[]{:S(2)}) async-start(bf16[8,32,8,128]{3,2,1,0:T(8,128)(2,1)} %broadcast_in_dim.45), calls=%async_computation.8 | async-start | bytes 1048576 | tf_op jit(solution)/shard_map/all_to_all | solution.py:11
  287.6 28.7 %copy-start.10 = (f32[128]{0:T(128)S(1)}, f32[128]{0:T(128)}, u32[]{:S(2)}) copy-start(f32[128]{0:T(128)} %param.41) | copy-start | bytes 1540
  296.7 19.4 %all-to-all-start.11 = ((bf16[8,512,128]{2,1,0:T(8,128)(2,1)}), bf16[8,512,128]{2,1,0:T(8,128)(2,1)S(1)}, u32[]{:S(2)}, u32[]{:S(2)}) async-start(bf16[8,512,128]{2,1,0:T(8,128)(2,1)} %broadcast_in_dim.47), calls=%async_computation.11 | async-start | bytes 2097152 | tf_op jit(solution)/shard_map/all_to_all | solution.py:11
